TPU v7x, 32 devices: a whole 2x2x4 slice. The times are simulated.
32 devices in a mesh: ep: 8 (over z, y), tp: 4 (over x, core).
Axes of the slice: x: 2, y: 2, z: 4, core: 2. Of those that a mesh axis runs over, the one named last changes fastest.
Arguments:
- queries: bfloat16 [2048, 768], P('ep', 'tp'), may hold values from -270 to 270
- key_rows: bfloat16 [2048, 256], P('ep', 'tp'), may hold values from -6 to 6
- value_rows: bfloat16 [2048, 256], P('ep', 'tp'), may hold values from -6 to 6
- sink_logits: float32 [12], P('tp'), may hold values from 2 to 6
- out_weight: bfloat16 [768, 2048], P('tp'), may hold values from -0.21875 to 0.21875
- mix_gain: float32 [2048], replicated, may hold values from 0.1 to 1.9
- moe_tokens: bfloat16 [4096, 2048], P(('ep', 'tp')), may hold values from -600 to 600
- moe_gain: float32 [2048], replicated, may hold values from 0.1 to 1.9
- routes: int32 [4096, 2], P(('ep', 'tp')), may hold values from 0 to 7, all different within a row; in each aligned block of 128 rows (0 to 127, 128 to 255, ...) at most 40 rows name the same one
- route_weights: float32 [4096, 2], P(('ep', 'tp')), may hold values from 0.25 to 1.5
- expert_gate: bfloat16 [8, 2048, 3584], P('ep', None, 'tp'), may hold values from -0.125 to 0.125
- expert_up: bfloat16 [8, 2048, 3584], P('ep', None, 'tp'), may hold values from -0.125 to 0.125
- expert_down: bfloat16 [8, 3584, 2048], P('ep', 'tp'), may hold values from -0.09375 to 0.09375
Outputs:
- mixed: bfloat16 [2048, 2048], P(('ep', 'tp'))
- moe_out: bfloat16 [4096, 2048], P(('ep', 'tp'))
Inputs may be any that keep to these rules, and one draw needn't show every extreme that they name: `routes`: each row names 2 different experts. In the rows of one device no expert is named more than 40 times, and in every draw some device names some expert exactly 40 times.
All inputs are finite; a program needn't handle non-finite values.
Results may differ from a plain program's by a relative error of at most 0.012.
Values may be sent and summed in bfloat16 or wider, within the bound.
A program may use at most 128 MiB of HBM per device.

v0:
```python
import jax
import jax.numpy as jnp
from jax import lax
from jax.sharding import PartitionSpec as P

HDIM = 64
WINDOW = 128


norm_eps = 1e-06
masked_value = -1e30


def shifted(shard, axis, by):
    size = lax.axis_size(axis)
    pairs = [(i, i + by) for i in range(size) if 0 <= i + by < size]
    return lax.ppermute(shard, axis, pairs)


def rms_scale(rows_in, gain):
    squares = jnp.mean(rows_in * rows_in, axis=-1, keepdims=True)
    return rows_in * lax.rsqrt(squares + norm_eps) * gain


def mixer(queries, key_rows, value_rows, sink_logits, out_weight, mix_gain):
    tok_rows = queries.shape[0]
    kv_local = key_rows.shape[1] // HDIM
    group_size = queries.shape[1] // key_rows.shape[1]
    rim_rows = (key_rows[tok_rows - WINDOW :], value_rows[tok_rows - WINDOW :])
    prev_keys, prev_values = shifted((rim_rows[0], rim_rows[1]), "ep", 1)
    all_keys = jnp.concatenate([prev_keys, key_rows], axis=0).reshape(
        tok_rows + WINDOW, kv_local, HDIM
    )
    all_values = jnp.concatenate([prev_values, value_rows], axis=0).reshape(
        tok_rows + WINDOW, kv_local, HDIM
    )
    offset = lax.axis_index("ep") * tok_rows
    query_pos = offset + jnp.arange(tok_rows, dtype=jnp.int32)
    key_pos = offset - WINDOW + jnp.arange(tok_rows + WINDOW, dtype=jnp.int32)
    distance = query_pos[:, None] - key_pos[None, :]
    allowed = (distance >= 0) & (distance < WINDOW) & (key_pos >= 0)[None, :]
    grouped = queries.reshape(tok_rows, kv_local, group_size, HDIM)
    scores = jnp.einsum(
        "qkgd,jkd->kgqj", grouped, all_keys, preferred_element_type=jnp.float32
    ) * HDIM ** (-0.5)
    logits = jnp.where(allowed, scores, masked_value)
    sink_logit = sink_logits.reshape(kv_local, group_size)[:, :, None, None]
    top_value = jnp.maximum(jnp.max(logits, axis=-1, keepdims=True), sink_logit)
    exponent = jnp.exp(logits - top_value)
    denominator = jnp.sum(exponent, axis=-1, keepdims=True) + jnp.exp(sink_logit - top_value)
    probs = (exponent / denominator).astype(jnp.bfloat16)
    attended = jnp.einsum("kgqj,jkd->qkgd", probs, all_values, preferred_element_type=jnp.float32)
    attended = attended.astype(jnp.bfloat16).reshape(tok_rows, -1)
    projected = lax.psum_scatter(
        jnp.dot(attended, out_weight, preferred_element_type=jnp.float32).astype(jnp.bfloat16),
        "tp",
        scatter_dimension=0,
        tiled=True,
    ).astype(jnp.float32)
    return rms_scale(projected, mix_gain).astype(jnp.bfloat16)


def slot_places(route_rows, experts):
    blocks, tok_rows, top_count = route_rows.shape
    flat_routes = route_rows.reshape(blocks, tok_rows * top_count)
    onehot = (
        flat_routes[:, :, None] == jnp.arange(experts, dtype=jnp.int32)[None, None, :]
    ).astype(jnp.int32)
    earlier = jnp.cumsum(onehot, axis=1) - onehot
    slot_rank = jnp.sum(earlier * onehot, axis=2)
    return (slot_rank * experts + flat_routes).reshape(blocks, tok_rows, top_count)


def dispatch_matrix(slot_place, slots):
    targets = jnp.arange(slots, dtype=jnp.int32)
    hits = (slot_place[:, None, :, :] == targets[None, :, None, None]).astype(jnp.float32)
    return jnp.sum(hits, axis=3).astype(jnp.bfloat16)


def routed_experts(
    moe_tokens, moe_gain, routes, route_weights, expert_gate, expert_up, expert_down
):
    tok_rows, width = moe_tokens.shape
    top_count = routes.shape[1]
    experts = lax.axis_size("ep")
    capacity = tok_rows * top_count * 5 // (4 * experts)
    normed = rms_scale(moe_tokens.astype(jnp.float32), moe_gain).astype(jnp.bfloat16)
    gate_weight = expert_gate[0]
    up_weight = expert_up[0]
    down_weight = expert_down[0]
    slot_place = slot_places(routes[None], experts)
    select_rows = dispatch_matrix(slot_place, capacity * experts)[0]
    outgoing = jnp.dot(select_rows, normed, preferred_element_type=jnp.float32)
    outgoing = outgoing.astype(jnp.bfloat16).reshape(capacity, experts, width)
    slot_rows = lax.all_gather(
        lax.all_to_all(outgoing, "ep", split_axis=1, concat_axis=1, tiled=True),
        "tp",
        axis=0,
        tiled=True,
    )
    gate_value = jnp.dot(slot_rows, gate_weight, preferred_element_type=jnp.float32)
    up_value = jnp.dot(slot_rows, up_weight, preferred_element_type=jnp.float32)
    hidden = (jax.nn.silu(gate_value) * up_value).astype(jnp.bfloat16)
    summed = lax.psum_scatter(
        jnp.dot(hidden, down_weight, preferred_element_type=jnp.float32).astype(jnp.bfloat16),
        "tp",
        scatter_dimension=0,
        tiled=True,
    )
    returned = lax.all_to_all(summed, "ep", split_axis=1, concat_axis=1, tiled=True)
    flat_returned = returned.reshape(capacity * experts, width)
    picked = flat_returned[slot_place[0]]
    combined = jnp.sum(route_weights[:, :, None] * picked.astype(jnp.float32), axis=1)
    return combined.astype(jnp.bfloat16)


def shards(
    queries,
    key_rows,
    value_rows,
    sink_logits,
    out_weight,
    mix_gain,
    moe_tokens,
    moe_gain,
    routes,
    route_weights,
    expert_gate,
    expert_up,
    expert_down,
):
    mixed = mixer(queries, key_rows, value_rows, sink_logits, out_weight, mix_gain)
    moe_out = routed_experts(
        moe_tokens, moe_gain, routes, route_weights, expert_gate, expert_up, expert_down
    )
    return (mixed, moe_out)


def solution(mesh):
    return jax.shard_map(
        shards,
        mesh=mesh,
        in_specs=(
            P("ep", "tp"),
            P("ep", "tp"),
            P("ep", "tp"),
            P("tp"),
            P("tp", None),
            P(),
            P(("ep", "tp"), None),
            P(),
            P(("ep", "tp"), None),
            P(("ep", "tp"), None),
            P("ep", None, "tp"),
            P("ep", None, "tp"),
            P("ep", "tp", None),
        ),
        out_specs=(P(("ep", "tp"), None), P(("ep", "tp"), None)),
        check_vma=False,
    )
```

profile of v0, /device:TPU:0, one launch (start us, length us, event | category | flops | bytes accessed | tf_op | source)
XLA Modules:
  0.0 227.5 jit_solution(6679655546497340957)
XLA Ops:
  7.2 0.0 copy-start
  7.2 0.0 all-gather.2.cloned.1.call-start
  7.2 0.8 copy.32
  8.1 0.1 eq.48
  8.2 0.6 reduce-window.6
  8.8 0.2 slice_reduce_fusion
  9.1 0.1 fusion.31
  9.2 0.1 mul.99
  9.3 0.1 copy.34
  9.4 0.1 convert_reduce_fusion
  9.5 1.2 fusion.10
  10.7 1.6 fusion.7
  12.3 0.7 copy.35
  13.1 38.5 %all_to_all.10 = bf16[40,8,2048]{2,0,1:T(8,128)(2,1)S(1)} all-to-all(bf16[40,8,2048]{2,0,1:T(8,128)(2,1)S(1)} %copy.35), channel_id=1, replica_groups=mesh['ep'=8,'tp'=4] {'ep'}, dimensions={1} | all-to-all | bytes 2621440 | tf_op jit(solution)/shard_map/all_to_all | solution.py:96
  51.6 1.8 copy.36
  53.3 0.0 all-gather.2.cloned.1.call-update
  53.4 0.0 reduce-scatter.5.cloned.1.call-start
  53.4 39.5 %all-gather.2.cloned.1.call-done = bf16[160,8,2048]{2,1,0:T(8,128)(2,1)} async-done(((bf16[40,8,2048]{2,1,0:T(8,128)(2,1)}), bf16[160,8,2048]{2,1,0:T(8,128)(2,1)}) %all-gather.2.cloned.1.call-update) | async-done | bytes 5242896 | tf_op jit(solution)/shard_map/all_gather | solution.py:95
  92.9 10.0 %fusion.1 = f32[160,8,896]{2,1,0:T(8,128)} fusion(bf16[160,8,2048]{2,1,0:T(8,128)(2,1)} %all-gather.2.cloned.1.call-done, bf16[1,2048,896]{2,1,0:T(8,128)(2,1)} %param.24), kind=kOutput, calls=%fused_computation.4 | convolution fusion | flops 4697620480 | bytes 13500416 | tf_op jit(solution)/shard_map/dot_general | solution.py:102
  102.9 17.3 %convolution_convert_fusion = bf16[160,8,2048]{2,1,0:T(8,128)(2,1)} fusion(bf16[1,896,2048]{2,1,0:T(8,128)(2,1)} %param.25, f32[160,8,896]{2,1,0:T(8,128)} %fusion.1, bf16[160,8,2048]{2,1,0:T(8,128)(2,1)} %all-gather.2.cloned.1.call-done, bf16[1,2048,896]{2,1,0:T(8,128)(2,1)} %param.23), kind=kOutput, calls=%fused_computation.2 | convolution fusion | flops 9404743680 | bytes 22413312 | tf_op jit(solution)/shard_map/dot_general | solution.py:105
  120.2 0.0 copy-start.4
  120.3 0.0 reduce-scatter.5.cloned.1.call-update
  120.3 0.0 reduce-scatter.3.cloned.1.call-start
  120.3 0.7 copy-done.2
  121.0 3.4 %collective-permute-start.1 = (bf16[128,64]{0,1:T(8,128)(2,1)S(1)}, bf16[128,64]{0,1:T(8,128)(2,1)S(1)}, u32[]{:S(2)}, u32[]{:S(2)}) collective-permute-start(bf16[128,64]{0,1:T(8,128)(2,1)S(1)} %slice.13), channel_id=1, source_target_pairs={{0,4},{4,8},{8,12},{12,16},{16,20},{20,24},{24,28},{1,5},{5,9},{9,... | collective-permute-start | bytes 49160 | tf_op jit(solution)/shard_map/ppermute | solution.py:17
  124.4 3.6 %collective-permute-start = (bf16[128,64]{0,1:T(8,128)(2,1)S(1)}, bf16[128,64]{0,1:T(8,128)(2,1)S(1)}, u32[]{:S(2)}, u32[]{:S(2)}) collective-permute-start(bf16[128,64]{0,1:T(8,128)(2,1)S(1)} %slice.12), channel_id=1, source_target_pairs={{0,4},{4,8},{8,12},{12,16},{16,20},{20,24},{24,28},{1,5},{5,9},{9,... | collective-permute-start | bytes 49160 | tf_op jit(solution)/shard_map/ppermute | solution.py:17
  128.0 0.2 fusion.24
  128.2 0.4 fusion.35
  128.6 0.1 broadcast_maximum_fusion
  128.7 0.2 fusion.13
  128.8 0.1 exponential_add_fusion
  128.9 0.3 collective-permute-done
  129.2 0.3 convolution_convert_fusion.3
  129.6 1.5 convolution_convert_fusion.2
  131.0 0.0 reduce-scatter.3.cloned.1.call-update
  131.1 40.7 %reduce-scatter.5.cloned.1.call-done = bf16[40,8,2048]{2,1,0:T(8,128)(2,1)} async-done(((bf16[160,8,2048]{2,1,0:T(8,128)(2,1)}), bf16[40,8,2048]{2,1,0:T(8,128)(2,1)}) %reduce-scatter.5.cloned.1.call-update) | async-done | bytes 1310736 | tf_op jit(solution)/shard_map/reduce_scatter | solution.py:104
  171.8 3.1 %copy.37 = bf16[40,8,2048]{2,0,1:T(8,128)(2,1)} copy(bf16[40,8,2048]{2,1,0:T(8,128)(2,1)} %reduce-scatter.5.cloned.1.call-done) | data formatting | bytes 2621440 | tf_op jit(solution)/shard_map/reduce_scatter | solution.py:104
  174.9 5.5 %all-to-all-start.1 = ((bf16[40,8,2048]{2,0,1:T(8,128)(2,1)}), bf16[40,8,2048]{2,0,1:T(8,128)(2,1)S(1)}, u32[]{:S(2)}, u32[]{:S(2)}) async-start(bf16[40,8,2048]{2,0,1:T(8,128)(2,1)} %copy.37), calls=%async_computation.3 | async-start | bytes 2621440 | tf_op jit(solution)/shard_map/all_to_all | solution.py:110
  180.4 0.1 reshape.289
  180.6 0.1 copy.31
  180.7 18.5 %reduce-scatter.3.cloned.1.call-done = bf16[64,2048]{1,0:T(8,128)(2,1)} async-done(((bf16[256,2048]{1,0:T(8,128)(2,1)}), bf16[64,2048]{1,0:T(8,128)(2,1)}) %reduce-scatter.3.cloned.1.call-update) | async-done | bytes 262160 | tf_op jit(solution)/shard_map/reduce_scatter | solution.py:54
  199.2 1.1 fusion.17
  200.3 1.8 fusion.19
  202.1 9.6 %all-to-all-done.1 = bf16[40,8,2048]{2,0,1:T(8,128)(2,1)S(1)} async-done(((bf16[40,8,2048]{2,0,1:T(8,128)(2,1)}), bf16[40,8,2048]{2,0,1:T(8,128)(2,1)S(1)}, u32[]{:S(2)}, u32[]{:S(2)}) %all-to-all-start.1) | async-done | bytes 1310752 | tf_op jit(solution)/shard_map/all_to_all | solution.py:110
  211.6 0.7 copy.41
  212.3 2.3 %gather_fusion = bf16[256,2048]{1,0:T(8,128)(2,1)} fusion(bf16[320,2048]{1,0:T(8,128)(2,1)S(1)} %bitcast.65, s32[1024]{0:T(1024)S(1)} %pad_clamp_fusion), kind=kCustom, calls=%fused_computation | custom fusion | bytes 2098176 | tf_op jit(solution)/shard_map/gather | solution.py:112
  214.7 2.4 %reshape.297 = f32[128,2,2048]{2,1,0:T(2,128)S(1)} reshape(bf16[256,2048]{1,0:T(8,128)(2,1)} %gather_fusion) | data formatting | bytes 3145728 | tf_op jit(solution)/shard_map/convert_element_type | solution.py:113
  217.1 3.9 %multiply_reduce_fusion = bf16[128,2048]{1,0:T(8,128)(2,1)} fusion(f32[128,2,2048]{2,1,0:T(2,128)S(1)} %reshape.297, f32[128,2]{1,0:T(8,128)S(1)} %copy.31), kind=kLoop, calls=%fused_computation.11 | loop fusion | flops 786432 | bytes 2622464 | tf_op jit(solution)/shard_map/reduce_sum | solution.py:113
  (25 shorter events, 0.1 us)
Async XLA Ops:
  7.2 122.4 %copy-start = (bf16[192,2048]{1,0:T(8,128)(2,1)S(1)}, bf16[192,2048]{1,0:T(8,128)(2,1)}, u32[]{:S(2)}) copy-start(bf16[192,2048]{1,0:T(8,128)(2,1)} %param.17) | copy-start | bytes 2359300
  7.2 85.8 %all-gather.2.cloned.1.call-start = ((), (), s32[]{:S(2)}) async-start(), calls=%async_computation.5 | async-start | bytes 6553600 | tf_op jit(solution)/shard_map/all_gather | solution.py:95
  53.4 118.4 %reduce-scatter.5.cloned.1.call-start = ((), (), s32[]{:S(2)}) async-start(), calls=%async_computation.6 | async-start | bytes 6553600 | tf_op jit(solution)/shard_map/reduce_scatter | solution.py:104
  120.2 0.8 copy-start.2
  120.2 4.1 %copy-start.3 = (bf16[256,64]{0,1:T(8,128)(2,1)S(1)}, bf16[256,64]{0,1:T(8,128)(2,1)}, u32[]{:S(2)}) copy-start(bf16[256,64]{0,1:T(8,128)(2,1)} %param.15) | copy-start | bytes 98308
  120.2 8.0 %copy-start.6 = (bf16[256,192]{0,1:T(8,128)(2,1)S(1)}, bf16[256,192]{0,1:T(8,128)(2,1)}, u32[]{:S(2)}) copy-start(bf16[256,192]{0,1:T(8,128)(2,1)} %param.13) | copy-start | bytes 294916
  120.2 8.3 %copy-start.4 = (f32[3]{0:T(128)S(1)}, f32[3]{0:T(128)}, u32[]{:S(2)}) copy-start(f32[3]{0:T(128)} %param.16) | copy-start | bytes 40
  120.3 78.9 %reduce-scatter.3.cloned.1.call-start = ((), (), s32[]{:S(2)}) async-start(), calls=%async_computation.4 | async-start | bytes 1310720 | tf_op jit(solution)/shard_map/reduce_scatter | solution.py:54
  121.0 7.2 %collective-permute-start.1 = (bf16[128,64]{0,1:T(8,128)(2,1)S(1)}, bf16[128,64]{0,1:T(8,128)(2,1)S(1)}, u32[]{:S(2)}, u32[]{:S(2)}) collective-permute-start(bf16[128,64]{0,1:T(8,128)(2,1)S(1)} %slice.13), channel_id=1, source_target_pairs={{0,4},{4,8},{8,12},{12,16},{16,20},{20,24},{24,28},{1,5},{5,9},{9,... | collective-permute-start | bytes 49160 | tf_op jit(solution)/shard_map/ppermute | solution.py:17
  124.4 4.8 %collective-permute-start = (bf16[128,64]{0,1:T(8,128)(2,1)S(1)}, bf16[128,64]{0,1:T(8,128)(2,1)S(1)}, u32[]{:S(2)}, u32[]{:S(2)}) collective-permute-start(bf16[128,64]{0,1:T(8,128)(2,1)S(1)} %slice.12), channel_id=1, source_target_pairs={{0,4},{4,8},{8,12},{12,16},{16,20},{20,24},{24,28},{1,5},{5,9},{9,... | collective-permute-start | bytes 49160 | tf_op jit(solution)/shard_map/ppermute | solution.py:17
  129.5 51.0 %copy-start.5 = (f32[128,2]{0,1:T(2,128)S(1)}, f32[128,2]{0,1:T(2,128)}, u32[]{:S(2)}) copy-start(f32[128,2]{0,1:T(2,128)} %param.22) | copy-start | bytes 3076
  131.0 69.2 %copy-start.1 = (f32[2048]{0:T(1024)S(1)}, f32[2048]{0:T(1024)}, u32[]{:S(2)}) copy-start(f32[2048]{0:T(1024)} %param.18) | copy-start | bytes 24580
  174.9 36.7 %all-to-all-start.1 = ((bf16[40,8,2048]{2,0,1:T(8,128)(2,1)}), bf16[40,8,2048]{2,0,1:T(8,128)(2,1)S(1)}, u32[]{:S(2)}, u32[]{:S(2)}) async-start(bf16[40,8,2048]{2,0,1:T(8,128)(2,1)} %copy.37), calls=%async_computation.3 | async-start | bytes 2621440 | tf_op jit(solution)/shard_map/all_to_all | solution.py:110
Sparse Core Ops, SparseCore 0:
  53.5 39.4 all-gather.1
  120.4 51.3 reduce-scatter.4
  174.3 24.7 reduce-scatter.2
where the time goes:
time: 228 us
  waiting for transfers between devices  109 us (48%)
  blocking collectives  38.5 us (17%)
  matrix products  31.1 us (14%)
  between operations  14 us (6%)
  local copies, waits for them, and re-layouts  13.4 us (6%)
  starting transfers between devices  12.6 us (6%)
  other arithmetic  9.38 us (4%)
    reduce_scatter x1, waiting for transfers between devices, routed_experts(): lax.psum_scatter(jnp.dot(hidden, down_weight, preferred_element_type=jnp....  40.7 us
    all_gather x1, waiting for transfers between devices, routed_experts(): lax.all_gather(lax.all_to_all(outgoing, 'ep', split_axis=1, concat_axis=1...  39.5 us
    all_to_all x1, blocking collectives, routed_experts(): lax.all_to_all(outgoing, 'ep', split_axis=1, concat_axis=1, tiled=True)  38.5 us
    reduce_scatter x1, waiting for transfers between devices, mixer(): lax.psum_scatter(jnp.dot(attended, out_weight, preferred_element_type=jnp...  18.5 us
    dot_general x1, matrix products, routed_experts(): jnp.dot(hidden, down_weight, preferred_element_type=jnp.float32)  17.3 us
    dot_general x1, matrix products, routed_experts(): up_value = jnp.dot(slot_rows, up_weight, preferred_element_type=jnp.float32)  9.97 us
    all_to_all x1, waiting for transfers between devices, routed_experts(): lax.all_to_all(summed, 'ep', split_axis=1, concat_axis=1, tiled=True)  9.55 us
    ppermute x2, starting transfers between devices, shifted(): return lax.ppermute(shard, axis, pairs)  6.93 us
  transfers between devices with their start and end apart: 6, of which 5 were waited for; matrix products, arithmetic and copies ran while one was open for 4% of the time, Pallas kernels for 0%

commit v1 on v0

v1 whole, which is shorter than its diff:
```python
import functools

import jax
import jax.numpy as jnp
from jax import lax
from jax.experimental import pallas as pl
from jax.experimental.pallas import tpu as pltpu
from jax.sharding import PartitionSpec as P

HDIM = 64
WINDOW = 128
MESH = pl.DeviceIdType.MESH


norm_eps = 1e-06
masked_value = -1e30


def rms_scale(rows_in, gain):
    squares = jnp.mean(rows_in * rows_in, axis=-1, keepdims=True)
    return rows_in * lax.rsqrt(squares + norm_eps) * gain


def slot_places(route_rows, experts, capacity):
    tok_rows, top_count = route_rows.shape
    flat_routes = route_rows.reshape(tok_rows * top_count)
    onehot = (flat_routes[:, None] == jnp.arange(experts, dtype=jnp.int32)[None, :]).astype(jnp.int32)
    earlier = jnp.cumsum(onehot, axis=0) - onehot
    slot_rank = jnp.sum(earlier * onehot, axis=1)
    return (flat_routes * capacity + slot_rank).reshape(tok_rows, top_count)


def far_first(n):
    return sorted(range(1, n), key=lambda k: -min(k, n - k))


def places():
    ep, tp = lax.axis_index("ep"), lax.axis_index("tp")
    pair = tp + 1 - 2 * lax.rem(tp, 2)
    cross = lax.rem(tp + 2, 4)
    return ep, tp, pair, cross


def enter(n, ep, tp, pair, cross):
    barrier = pltpu.get_barrier_semaphore()
    for k in range(1, n):
        pl.semaphore_signal(barrier, inc=1, device_id=(lax.rem(ep + k, n), tp), device_id_type=MESH)
    for other in (pair, cross):
        pl.semaphore_signal(barrier, inc=1, device_id=(ep, other), device_id_type=MESH)
    pl.semaphore_wait(barrier, n + 1)


def send(src, dst, send_sem, recv_sem, where):
    copy = pltpu.make_async_remote_copy(
        src_ref=src, dst_ref=dst, send_sem=send_sem, recv_sem=recv_sem,
        device_id=where, device_id_type=MESH,
    )
    copy.start()
    return copy


def dispatch_kernel(
    n, out_ref, q_ref, kv_ref, sink_ref, w_ref, gain_ref,
    slots, mixed_ref,
    kv_prev, part, mix_in, mix_sum, mix_x,
    send_d, recv_d, send_p, recv_p, send_x, recv_x, send_q, recv_q, send_m, recv_m,
):
    ep, tp, pair, cross = places()
    diag = lax.rem(pair + 2, 4)
    enter(n, ep, tp, pair, cross)
    tok_rows = kv_ref.shape[0]
    group_size = q_ref.shape[0]
    copies = []
    halo = send(
        kv_ref.at[pl.ds(tok_rows - WINDOW, WINDOW)], kv_prev,
        send_m.at[0], recv_m.at[0], (lax.rem(ep + 1, n), tp),
    )
    order = far_first(n)
    direct = {}
    own = out_ref.at[ep]
    crossed = {0: send(own, slots.at[2, 0], send_x.at[0], recv_x.at[0], (ep, cross))}
    for k in order:
        to = lax.rem(ep + k, n)
        direct[k] = send(out_ref.at[to], slots.at[0, k], send_d.at[k], recv_d.at[k], (to, tp))
    copies.append(send(own, slots.at[1, 0], send_p.at[0], recv_p.at[0], (ep, pair)))
    slots[0, 0] = out_ref[ep]

    halo.wait()
    rows = tok_rows + WINDOW
    kv = jnp.concatenate([kv_prev[...], kv_ref[...]], axis=0)
    row = lax.broadcasted_iota(jnp.int32, (tok_rows, rows), 0)
    col = lax.broadcasted_iota(jnp.int32, (tok_rows, rows), 1)
    distance = row - (col - WINDOW)
    key_pos = ep * tok_rows - WINDOW + col
    allowed = (distance >= 0) & (distance < WINDOW) & (key_pos >= 0)
    heads = []
    for g in range(group_size):
        scores = lax.dot_general(
            q_ref[g], kv, (((1,), (1,)), ((), ())), preferred_element_type=jnp.float32
        ) * HDIM ** (-0.5)
        logits = jnp.where(allowed, scores, masked_value)
        sink = sink_ref[g : g + 1, 0:1]
        top = jnp.maximum(jnp.max(logits, axis=-1, keepdims=True), sink)
        exponent = jnp.exp(logits - top)
        denominator = jnp.sum(exponent, axis=-1, keepdims=True) + jnp.exp(sink - top)
        probs = (exponent / denominator).astype(jnp.bfloat16)
        heads.append(jnp.dot(probs, kv, preferred_element_type=jnp.float32).astype(jnp.bfloat16))
    block = tok_rows // 4
    for b in range(4):
        total = None
        for g in range(group_size):
            term = jnp.dot(
                heads[g][b * block : (b + 1) * block], w_ref[g], preferred_element_type=jnp.float32
            )
            total = term if total is None else total + term
        part[b] = total.astype(jnp.bfloat16)
    to_sum = send(part.at[diag], mix_in.at[1], send_m.at[1], recv_m.at[1], (ep, pair))
    to_own = send(part.at[pair], mix_in.at[0], send_m.at[2], recv_m.at[2], (ep, pair))
    to_sum.wait()
    mix_sum[...] = (part[cross].astype(jnp.float32) + mix_in[1].astype(jnp.float32)).astype(jnp.bfloat16)
    over_x = send(mix_sum, mix_x, send_m.at[3], recv_m.at[3], (ep, cross))

    pending = [0]
    for k in order:
        direct[k].wait_recv()
        crossed[k] = send(slots.at[0, k], slots.at[2, k], send_x.at[k], recv_x.at[k], (ep, cross))
        copies.append(send(slots.at[0, k], slots.at[1, k], send_p.at[k], recv_p.at[k], (ep, pair)))
        pending.append(k)
    diagonal = []
    for i, k in enumerate(pending):
        crossed[k].wait_recv()
        diagonal.append(send(slots.at[2, k], slots.at[3, k], send_q.at[k], recv_q.at[k], (ep, pair)))
        if i == 1 or n == 1:
            to_own.wait()
            over_x.wait()
            projected = (
                part[tp].astype(jnp.float32) + mix_in[0].astype(jnp.float32) + mix_x[...].astype(jnp.float32)
            )
            mixed_ref[...] = rms_scale(projected, gain_ref[...]).astype(jnp.bfloat16)
    for copy in copies + diagonal:
        copy.wait()
    for k in order:
        direct[k].wait_send()
    for k in pending:
        crossed[k].wait_send()


def dispatch(outgoing, queries, kv, sinks, weight, gain):
    n, capacity, width = outgoing.shape
    tok_rows = kv.shape[0]
    block = tok_rows // 4
    vmem = pl.BlockSpec(memory_space=pltpu.VMEM)
    sems = pltpu.SemaphoreType.DMA
    return pl.pallas_call(
        functools.partial(dispatch_kernel, n),
        out_shape=(
            jax.ShapeDtypeStruct((4, n, capacity, width), jnp.bfloat16),
            jax.ShapeDtypeStruct((block, width), jnp.bfloat16),
        ),
        in_specs=[vmem] * 6,
        out_specs=(vmem, vmem),
        scratch_shapes=[
            pltpu.VMEM((WINDOW, kv.shape[1]), jnp.bfloat16),
            pltpu.VMEM((4, block, width), jnp.bfloat16),
            pltpu.VMEM((2, block, width), jnp.bfloat16),
            pltpu.VMEM((block, width), jnp.bfloat16),
            pltpu.VMEM((block, width), jnp.bfloat16),
        ]
        + [sems((n,))] * 8
        + [sems((4,))] * 2,
        compiler_params=pltpu.CompilerParams(collective_id=0, has_side_effects=True),
    )(outgoing, queries, kv, sinks, weight, gain)


def combine_kernel(
    n, y_ref, ret, pair_in, cross_out, cross_in, back_out,
    send_a, recv_a, send_b, recv_b, send_x, recv_x, send_r, recv_r,
):
    ep, tp, pair, cross = places()
    enter(n, ep, tp, pair, cross)
    order = far_first(n) + [0]
    first, second, crossed, back = {}, {}, {}, {}
    for k in order:
        first[k] = send(y_ref.at[3, k], pair_in.at[1, k], send_a.at[k], recv_a.at[k], (ep, pair))
    for k in order:
        second[k] = send(y_ref.at[1, k], pair_in.at[0, k], send_b.at[k], recv_b.at[k], (ep, pair))
    for k in order:
        first[k].wait_recv()
        cross_out[k] = (
            y_ref[2, k].astype(jnp.float32) + pair_in[1, k].astype(jnp.float32)
        ).astype(jnp.bfloat16)
        crossed[k] = send(cross_out.at[k], cross_in.at[k], send_x.at[k], recv_x.at[k], (ep, cross))
    for k in order:
        second[k].wait_recv()
        crossed[k].wait_recv()
        total = (
            y_ref[0, k].astype(jnp.float32)
            + pair_in[0, k].astype(jnp.float32)
            + cross_in[k].astype(jnp.float32)
        ).astype(jnp.bfloat16)
        if k == 0:
            ret[ep] = total
        else:
            back_out[k] = total
            to = lax.rem(ep + n - k, n)
            back[k] = send(back_out.at[k], ret.at[ep], send_r.at[k], recv_r.at[k], (to, tp))
    for k in order:
        if k:
            pltpu.make_async_remote_copy(
                src_ref=back_out.at[k], dst_ref=ret.at[lax.rem(ep + k, n)],
                send_sem=send_r.at[k], recv_sem=recv_r.at[k],
                device_id=(lax.rem(ep + n - k, n), tp), device_id_type=MESH,
            ).wait()
    for k in order:
        first[k].wait_send()
        second[k].wait_send()
        crossed[k].wait_send()


def combine(partial_rows):
    _, n, capacity, width = partial_rows.shape
    vmem = pl.BlockSpec(memory_space=pltpu.VMEM)
    sems = pltpu.SemaphoreType.DMA
    blocks = pltpu.VMEM((n, capacity, width), jnp.bfloat16)
    return pl.pallas_call(
        functools.partial(combine_kernel, n),
        out_shape=jax.ShapeDtypeStruct((n, capacity, width), jnp.bfloat16),
        in_specs=[vmem],
        out_specs=vmem,
        scratch_shapes=[pltpu.VMEM((2, n, capacity, width), jnp.bfloat16), blocks, blocks, blocks]
        + [sems((n,))] * 8,
        compiler_params=pltpu.CompilerParams(collective_id=1, has_side_effects=True),
    )(partial_rows)


def shards(
    queries,
    key_rows,
    value_rows,
    sink_logits,
    out_weight,
    mix_gain,
    moe_tokens,
    moe_gain,
    routes,
    route_weights,
    expert_gate,
    expert_up,
    expert_down,
):
    tok_rows, width = moe_tokens.shape
    top_count = routes.shape[1]
    experts = lax.axis_size("ep")
    capacity = tok_rows * top_count * 5 // (4 * experts)
    slots = capacity * experts

    normed = rms_scale(moe_tokens.astype(jnp.float32), moe_gain).astype(jnp.bfloat16)
    slot_place = slot_places(routes, experts, capacity)
    targets = jnp.arange(slots, dtype=jnp.int32)
    hits = (slot_place[None, :, :] == targets[:, None, None]).astype(jnp.float32)
    select_rows = jnp.sum(hits, axis=2).astype(jnp.bfloat16)
    outgoing = jnp.dot(select_rows, normed, preferred_element_type=jnp.float32)
    outgoing = outgoing.astype(jnp.bfloat16).reshape(experts, capacity, width)

    group_size = queries.shape[1] // HDIM
    q = jnp.transpose(queries.reshape(-1, group_size, HDIM), (1, 0, 2))
    q = jnp.pad(q, ((0, 0), (0, 0), (0, HDIM)))
    kv = jnp.concatenate([key_rows, value_rows], axis=1)
    weight = jnp.pad(out_weight.reshape(group_size, HDIM, width), ((0, 0), (HDIM, 0), (0, 0)))
    sinks = jnp.broadcast_to(sink_logits[:, None], (group_size, 128))
    slot_rows, mixed = dispatch(outgoing, q, kv, sinks, weight, mix_gain[None])

    slot_rows = slot_rows.reshape(4 * slots, width)
    gate_value = jnp.dot(slot_rows, expert_gate[0], preferred_element_type=jnp.float32)
    up_value = jnp.dot(slot_rows, expert_up[0], preferred_element_type=jnp.float32)
    hidden = (jax.nn.silu(gate_value) * up_value).astype(jnp.bfloat16)
    blocks = jnp.dot(hidden, expert_down[0], preferred_element_type=jnp.float32).astype(jnp.bfloat16)
    returned = combine(blocks.reshape(4, experts, capacity, width)).reshape(slots, width)

    spots = slot_place[:, :, None] == targets[None, None, :]
    spread = jnp.sum(jnp.where(spots, route_weights[:, :, None], 0.0), axis=1)
    high = spread.astype(jnp.bfloat16)
    low = (spread - high.astype(jnp.float32)).astype(jnp.bfloat16)
    combined = jnp.dot(high, returned, preferred_element_type=jnp.float32) + jnp.dot(
        low, returned, preferred_element_type=jnp.float32
    )
    return (mixed, combined.astype(jnp.bfloat16))


def solution(mesh):
    return jax.shard_map(
        shards,
        mesh=mesh,
        in_specs=(
            P("ep", "tp"),
            P("ep", "tp"),
            P("ep", "tp"),
            P("tp"),
            P("tp", None),
            P(),
            P(("ep", "tp"), None),
            P(),
            P(("ep", "tp"), None),
            P(("ep", "tp"), None),
            P("ep", None, "tp"),
            P("ep", None, "tp"),
            P("ep", "tp", None),
        ),
        out_specs=(P(("ep", "tp"), None), P(("ep", "tp"), None)),
        check_vma=False,
    )
```

time: 228 us -> 149 us (0.65)
  waiting for transfers between devices: 109 us -> 0 us
  Pallas kernels: 0 us -> 103 us
  blocking collectives: 38.5 us -> 0 us
  between operations: 14 us -> 0.76 us
  starting transfers between devices: 12.6 us -> 0 us
  local copies, waits for them, and re-layouts: 13.4 us -> 7.03 us
  other arithmetic: 9.38 us -> 3.55 us
  matrix products: 31.1 us -> 34.6 us
    pallas_call x0 -> x2, Pallas kernels: none -> 103 us  [the longest x1 57.6 us: dispatch(): pl.pallas_call(functools.partial(dispatch_kernel, n), out_shape=(jax.Shap...]
    reduce_scatter x2 -> x0, waiting for transfers between devices: 59.2 us -> none  [the longest x1 40.7 us: routed_experts(): lax.psum_scatter(jnp.dot(hidden, down_weight, preferred_element_type=jnp....]
    all_gather x1 -> x0, waiting for transfers between devices: 39.5 us -> none  [routed_experts(): lax.all_gather(lax.all_to_all(outgoing, 'ep', split_axis=1, concat_axis=1...]
    all_to_all x1 -> x0, blocking collectives: 38.5 us -> none  [routed_experts(): lax.all_to_all(outgoing, 'ep', split_axis=1, concat_axis=1, tiled=True)]
    all_to_all x1 -> x0, waiting for transfers between devices: 9.55 us -> none  [routed_experts(): lax.all_to_all(summed, 'ep', split_axis=1, concat_axis=1, tiled=True)]
    ppermute x2 -> x0, starting transfers between devices: 6.93 us -> none  [shifted(): return lax.ppermute(shard, axis, pairs)]
    all_to_all x1 -> x0, starting transfers between devices: 5.52 us -> none  [routed_experts(): lax.all_to_all(summed, 'ep', split_axis=1, concat_axis=1, tiled=True)]
    reduce_sum x4 -> x3, other arithmetic: 4.26 us -> 0.17 us  [the longest x1 0.09 us: slot_places(): slot_rank = jnp.sum(earlier * onehot, axis=1)]
  transfers between devices with their start and end apart: 6 -> 0, of which waited for: 5 -> 0; matrix products, arithmetic and copies ran while one was open for 4% -> 0% of each run, Pallas kernels for 0% -> 0%
where the time goes in v1:
time: 149 us
  Pallas kernels  103 us (69%)
  matrix products  34.6 us (23%)
  local copies, waits for them, and re-layouts  7.03 us (5%)
  other arithmetic  3.55 us (2%)
    pallas_call x1, Pallas kernels, dispatch(): pl.pallas_call(functools.partial(dispatch_kernel, n), out_shape=(jax.Shap...  57.6 us
    pallas_call x1, Pallas kernels, combine(): pl.pallas_call(functools.partial(combine_kernel, n), out_shape=jax.ShapeD...  45 us
    dot_general x1, matrix products, shards(): jnp.dot(hidden, expert_down[0], preferred_element_type=jnp.float32)  17.6 us
    dot_general x1, matrix products, shards(): jnp.dot(slot_rows, expert_gate[0], preferred_element_type=jnp.float32)  9.99 us

profile of v1, /device:TPU:0, one launch (start us, length us, event | category | flops | bytes accessed | tf_op | source)
XLA Modules:
  0.0 148.5 jit_solution(11530620279300156879)
XLA Ops:
  0.6 0.0 copy-start.2
  0.6 0.0 copy-start.4
  0.7 0.0 copy-start
  0.7 1.3 fusion.5
  2.0 0.8 copy.37
  2.8 0.1 eq.55
  2.9 0.6 reduce-window.6
  3.5 0.2 slice_reduce_fusion
  3.8 0.1 eq.51
  3.9 0.1 fusion.16
  4.0 0.1 reduce_sum.39
  4.1 0.1 copy.39
  4.2 0.7 multiply_add_fusion
  5.0 2.7 %convolution_convert_fusion.1 = bf16[320,2048]{1,0:T(8,128)(2,1)} fusion(bf16[128,2048]{1,0:T(8,128)(2,1)} %param.19, f32[2048]{0:T(1024)} %param.20, f32[128]{0:T(128)S(1)} %add_rsqrt_fusion, bf16[320,128]{1,0:T(8,128)(2,1)S(1)} %convert_reduce_fusion), kind=kOutput, calls=%fused_computation.6 | convolution fusion | flops 169476096 | bytes 1925632 | tf_op jit(solution)/shard_map/dot_general | solution.py:262
  7.6 1.1 copy.40
  8.7 0.7 pad.8.q_ref
  9.4 0.9 copy.42
  10.3 0.0 copy-done.2
  10.3 0.1 copy.41
  10.4 0.7 pad_maximum_fusion.kv_ref
  11.2 0.0 copy-done.4
  11.2 0.7 broadcast_in_dim.12.sink_ref
  11.8 0.0 copy-done
  11.8 1.4 pad.9.w_ref
  13.2 57.6 %shard_map.140 = (bf16[4,8,40,2048]{3,2,1,0:T(8,128)(2,1)}, bf16[64,2048]{1,0:T(8,128)(2,1)}) custom-call(bf16[8,40,2048]{2,1,0:T(8,128)(2,1)} %bitcast.42, bf16[3,256,128]{2,1,0:T(8,128)(2,1)} %pad.8.q_ref, bf16[256,128]{1,0:T(8,128)(2,1)} %pad_maximum_fusion.kv_ref, f32[3,128]{1,0:T(4,128)} %broadcast_in_dim.12.sink_ref, bf16[3,128,2048]{2,1,0:T(8,128)(2,1)} %pad.9.w_ref, ...), custom_call_target="tpu_custom_call" | custom-call | tf_op jit(solution)/shard_map/pallas_call | solution.py:154
  70.8 10.0 %fusion.2 = f32[1280,896]{1,0:T(8,128)} fusion(bf16[1280,2048]{1,0:T(8,128)(2,1)} %bitcast.47, bf16[1,2048,896]{2,1,0:T(8,128)(2,1)} %param.23), kind=kOutput, calls=%fused_computation.4 | convolution fusion | flops 4697620480 | bytes 13500416 | tf_op jit(solution)/shard_map/dot_general | solution.py:274
  80.8 17.6 %convolution_convert_fusion = bf16[1280,2048]{1,0:T(8,128)(2,1)} fusion(bf16[1,896,2048]{2,1,0:T(8,128)(2,1)} %param.25, f32[1280,896]{1,0:T(8,128)} %fusion.2, bf16[1280,2048]{1,0:T(8,128)(2,1)} %bitcast.48, bf16[1,2048,896]{2,1,0:T(8,128)(2,1)} %param.24), kind=kOutput, calls=%fused_computation | convolution fusion | flops 9404743680 | bytes 22413312 | tf_op jit(solution)/shard_map/dot_general | solution.py:277
  98.4 0.0 copy-start.3
  98.4 45.0 %shard_map.141 = bf16[8,40,2048]{2,1,0:T(8,128)(2,1)} custom-call(bf16[4,8,40,2048]{3,2,1,0:T(8,128)(2,1)} %bitcast.41), custom_call_target="tpu_custom_call" | custom-call | tf_op jit(solution)/shard_map/pallas_call | solution.py:225
  143.3 0.0 copy-start.1
  143.4 0.0 copy-done.3
  143.4 1.8 %fusion.13 = f32[128,2048]{1,0:T(8,128)S(1)} fusion(bf16[320,2048]{1,0:T(8,128)(2,1)} %bitcast.39, f32[128,320]{0,1:T(8,128)S(1)} %select_reduce_fusion), kind=kOutput, calls=%fused_computation.24 | convolution fusion | flops 167813120 | bytes 2523136 | tf_op jit(solution)/shard_map/dot_general | solution.py:284
  145.2 2.6 %fusion.4 = bf16[128,2048]{1,0:T(8,128)(2,1)} fusion(f32[128,2048]{1,0:T(8,128)S(1)} %fusion.13, bf16[320,2048]{1,0:T(8,128)(2,1)} %bitcast.40, f32[128,320]{0,1:T(8,128)S(1)} %select_reduce_fusion), kind=kOutput, calls=%fused_computation.8 | convolution fusion | flops 168460288 | bytes 3047424 | tf_op jit(solution)/shard_map/dot_general | solution.py:284
  147.8 0.0 copy-done.1
  147.8 0.7 copy.44
  (6 shorter events, 0.1 us)
Async XLA Ops:
  0.6 9.7 %copy-start.2 = (bf16[256,64]{0,1:T(8,128)(2,1)S(1)}, bf16[256,64]{0,1:T(8,128)(2,1)}, u32[]{:S(2)}) copy-start(bf16[256,64]{0,1:T(8,128)(2,1)} %param.14) | copy-start | bytes 98308
  0.6 10.5 %copy-start.4 = (f32[3]{0:T(128)S(1)}, f32[3]{0:T(128)}, u32[]{:S(2)}) copy-start(f32[3]{0:T(128)} %param.16) | copy-start | bytes 40
  0.7 11.2 %copy-start = (bf16[192,2048]{1,0:T(8,128)(2,1)S(1)}, bf16[192,2048]{1,0:T(8,128)(2,1)}, u32[]{:S(2)}) copy-start(bf16[192,2048]{1,0:T(8,128)(2,1)} %param.17) | copy-start | bytes 2359300
  98.4 45.0 %copy-start.3 = (f32[128,2]{0,1:T(2,128)S(1)}, f32[128,2]{0,1:T(2,128)}, u32[]{:S(2)}) copy-start(f32[128,2]{0,1:T(2,128)} %param.22) | copy-start | bytes 3076
  143.3 4.5 %copy-start.1 = (bf16[64,2048]{1,0:T(8,128)(2,1)S(1)}, bf16[64,2048]{1,0:T(8,128)(2,1)}, u32[]{:S(2)}) copy-start(bf16[64,2048]{1,0:T(8,128)(2,1)} %get-tuple-element.8) | copy-start | bytes 786436

commit v2 on v1

--- a/solution.py
+++ b/solution.py
@@ -94,7 +94,8 @@
     key_pos = ep * tok_rows - WINDOW + col
     allowed = (distance >= 0) & (distance < WINDOW) & (key_pos >= 0)
     heads = []
-    for g in range(group_size):
+
+    def attend(g):
         scores = lax.dot_general(
             q_ref[g], kv, (((1,), (1,)), ((), ())), preferred_element_type=jnp.float32
         ) * HDIM ** (-0.5)
@@ -105,20 +106,28 @@
         denominator = jnp.sum(exponent, axis=-1, keepdims=True) + jnp.exp(sink - top)
         probs = (exponent / denominator).astype(jnp.bfloat16)
         heads.append(jnp.dot(probs, kv, preferred_element_type=jnp.float32).astype(jnp.bfloat16))
+
     block = tok_rows // 4
-    for b in range(4):
-        total = None
-        for g in range(group_size):
-            term = jnp.dot(
-                heads[g][b * block : (b + 1) * block], w_ref[g], preferred_element_type=jnp.float32
-            )
-            total = term if total is None else total + term
-        part[b] = total.astype(jnp.bfloat16)
-    to_sum = send(part.at[diag], mix_in.at[1], send_m.at[1], recv_m.at[1], (ep, pair))
-    to_own = send(part.at[pair], mix_in.at[0], send_m.at[2], recv_m.at[2], (ep, pair))
-    to_sum.wait()
-    mix_sum[...] = (part[cross].astype(jnp.float32) + mix_in[1].astype(jnp.float32)).astype(jnp.bfloat16)
-    over_x = send(mix_sum, mix_x, send_m.at[3], recv_m.at[3], (ep, cross))
+    mixing = {}
+
+    def project():
+        for b in range(4):
+            total = None
+            for g in range(group_size):
+                term = jnp.dot(
+                    heads[g][b * block : (b + 1) * block], w_ref[g], preferred_element_type=jnp.float32
+                )
+                total = term if total is None else total + term
+            part[b] = total.astype(jnp.bfloat16)
+        mixing["sum"] = send(part.at[diag], mix_in.at[1], send_m.at[1], recv_m.at[1], (ep, pair))
+        mixing["own"] = send(part.at[pair], mix_in.at[0], send_m.at[2], recv_m.at[2], (ep, pair))
+
+    def cross_part():
+        mixing["sum"].wait()
+        mix_sum[...] = (part[cross].astype(jnp.float32) + mix_in[1].astype(jnp.float32)).astype(jnp.bfloat16)
+        mixing["x"] = send(mix_sum, mix_x, send_m.at[3], recv_m.at[3], (ep, cross))
+
+    pieces = [functools.partial(attend, g) for g in range(group_size)] + [project, cross_part]
 
     pending = [0]
     for k in order:
@@ -126,13 +135,17 @@
         crossed[k] = send(slots.at[0, k], slots.at[2, k], send_x.at[k], recv_x.at[k], (ep, cross))
         copies.append(send(slots.at[0, k], slots.at[1, k], send_p.at[k], recv_p.at[k], (ep, pair)))
         pending.append(k)
+        if pieces:
+            pieces.pop(0)()
+    for piece in pieces:
+        piece()
     diagonal = []
     for i, k in enumerate(pending):
         crossed[k].wait_recv()
         diagonal.append(send(slots.at[2, k], slots.at[3, k], send_q.at[k], recv_q.at[k], (ep, pair)))
         if i == 1 or n == 1:
-            to_own.wait()
-            over_x.wait()
+            mixing["own"].wait()
+            mixing["x"].wait()
             projected = (
                 part[tp].astype(jnp.float32) + mix_in[0].astype(jnp.float32) + mix_x[...].astype(jnp.float32)
             )
@@ -173,23 +186,38 @@
 
 
 def combine_kernel(
-    n, y_ref, ret, pair_in, cross_out, cross_in, back_out,
+    n, h_ref, down_ref, ret, y_ref, pair_in, cross_out, cross_in, back_out,
     send_a, recv_a, send_b, recv_b, send_x, recv_x, send_r, recv_r,
 ):
     ep, tp, pair, cross = places()
     enter(n, ep, tp, pair, cross)
     order = far_first(n) + [0]
+    capacity, width = ret.shape[1:]
+    tile = width // 4
     first, second, crossed, back = {}, {}, {}, {}
+
+    def down(r):
+        for c in range(0, width, tile):
+            product = jnp.dot(
+                h_ref[r], down_ref[:, c : c + tile], preferred_element_type=jnp.float32
+            ).astype(jnp.bfloat16)
+            for k in range(n):
+                y_ref[r, k, :, c : c + tile] = product[k * capacity : (k + 1) * capacity]
+
+    down(3)
     for k in order:
         first[k] = send(y_ref.at[3, k], pair_in.at[1, k], send_a.at[k], recv_a.at[k], (ep, pair))
-    for k in order:
-        second[k] = send(y_ref.at[1, k], pair_in.at[0, k], send_b.at[k], recv_b.at[k], (ep, pair))
+    down(2)
     for k in order:
         first[k].wait_recv()
         cross_out[k] = (
             y_ref[2, k].astype(jnp.float32) + pair_in[1, k].astype(jnp.float32)
         ).astype(jnp.bfloat16)
         crossed[k] = send(cross_out.at[k], cross_in.at[k], send_x.at[k], recv_x.at[k], (ep, cross))
+    down(1)
+    for k in order:
+        second[k] = send(y_ref.at[1, k], pair_in.at[0, k], send_b.at[k], recv_b.at[k], (ep, pair))
+    down(0)
     for k in order:
         second[k].wait_recv()
         crossed[k].wait_recv()
@@ -217,20 +245,23 @@
         crossed[k].wait_send()
 
 
-def combine(partial_rows):
-    _, n, capacity, width = partial_rows.shape
+def combine(hidden, down_weight, n):
+    capacity, width = hidden.shape[1] // n, down_weight.shape[1]
     vmem = pl.BlockSpec(memory_space=pltpu.VMEM)
     sems = pltpu.SemaphoreType.DMA
     blocks = pltpu.VMEM((n, capacity, width), jnp.bfloat16)
     return pl.pallas_call(
         functools.partial(combine_kernel, n),
         out_shape=jax.ShapeDtypeStruct((n, capacity, width), jnp.bfloat16),
-        in_specs=[vmem],
+        in_specs=[vmem, vmem],
         out_specs=vmem,
-        scratch_shapes=[pltpu.VMEM((2, n, capacity, width), jnp.bfloat16), blocks, blocks, blocks]
+        scratch_shapes=[
+            pltpu.VMEM((4, n, capacity, width), jnp.bfloat16),
+            pltpu.VMEM((2, n, capacity, width), jnp.bfloat16),
+            blocks, blocks, blocks]
         + [sems((n,))] * 8,
         compiler_params=pltpu.CompilerParams(collective_id=1, has_side_effects=True),
-    )(partial_rows)
+    )(hidden, down_weight)
 
 
 def shards(
@@ -274,8 +305,7 @@
     gate_value = jnp.dot(slot_rows, expert_gate[0], preferred_element_type=jnp.float32)
     up_value = jnp.dot(slot_rows, expert_up[0], preferred_element_type=jnp.float32)
     hidden = (jax.nn.silu(gate_value) * up_value).astype(jnp.bfloat16)
-    blocks = jnp.dot(hidden, expert_down[0], preferred_element_type=jnp.float32).astype(jnp.bfloat16)
-    returned = combine(blocks.reshape(4, experts, capacity, width)).reshape(slots, width)
+    returned = combine(hidden.reshape(4, slots, -1), expert_down[0], experts).reshape(slots, width)
 
     spots = slot_place[:, :, None] == targets[None, None, :]
     spread = jnp.sum(jnp.where(spots, route_weights[:, :, None], 0.0), axis=1)

time: 149 us -> 141 us (0.946)
  matrix products: 34.6 us -> 22.8 us
  Pallas kernels: 103 us -> 107 us
    dot_general x1, matrix products: 17.6 us -> 6.92 us  [shards(): jnp.dot(slot_rows, expert_up[0], preferred_element_type=jnp.float32)]
    pallas_call x1, Pallas kernels: 57.6 us -> 63.2 us  [dispatch(): pl.pallas_call(functools.partial(dispatch_kernel, n), out_shape=(jax.Shap...]
    pallas_call x1, Pallas kernels: 45 us -> 43.5 us  [combine(): pl.pallas_call(functools.partial(combine_kernel, n), out_shape=jax.ShapeD...]
where the time goes in v2:
time: 141 us
  Pallas kernels  107 us (76%)
  matrix products  22.8 us (16%)
  local copies, waits for them, and re-layouts  7.02 us (5%)
  other arithmetic  3.55 us (3%)
    pallas_call x1, Pallas kernels, dispatch(): pl.pallas_call(functools.partial(dispatch_kernel, n), out_shape=(jax.Shap...  63.2 us
    pallas_call x1, Pallas kernels, combine(): pl.pallas_call(functools.partial(combine_kernel, n), out_shape=jax.ShapeD...  43.5 us
    dot_general x1, matrix products, shards(): jnp.dot(slot_rows, expert_gate[0], preferred_element_type=jnp.float32)  8.74 us
    dot_general x1, matrix products, shards(): jnp.dot(slot_rows, expert_up[0], preferred_element_type=jnp.float32)  6.92 us

profile of v2, /device:TPU:0, one launch (start us, length us, event | category | flops | bytes accessed | tf_op | source)
XLA Modules:
  0.0 140.8 jit_solution(5932872774327450651)
XLA Ops:
  0.6 0.0 copy-start.2
  0.6 0.0 copy-start.4
  0.7 0.0 copy-start
  0.7 1.3 fusion.4
  2.0 0.8 copy.37
  2.8 0.1 eq.55
  2.9 0.6 reduce-window.6
  3.5 0.2 slice_reduce_fusion
  3.8 0.1 eq.51
  3.9 0.1 fusion.15
  4.0 0.1 reduce_sum.39
  4.1 0.1 copy.39
  4.2 0.7 multiply_add_fusion
  5.0 2.7 %convolution_convert_fusion = bf16[320,2048]{1,0:T(8,128)(2,1)} fusion(bf16[128,2048]{1,0:T(8,128)(2,1)} %param.19, f32[2048]{0:T(1024)} %param.20, f32[128]{0:T(128)S(1)} %add_rsqrt_fusion, bf16[320,128]{1,0:T(8,128)(2,1)S(1)} %convert_reduce_fusion), kind=kOutput, calls=%fused_computation.4 | convolution fusion | flops 169476096 | bytes 1925632 | tf_op jit(solution)/shard_map/dot_general | solution.py:293
  7.6 1.1 copy.40
  8.7 0.7 pad.8.q_ref
  9.4 0.9 copy.42
  10.3 0.0 copy-done.2
  10.3 0.1 copy.41
  10.4 0.7 pad_maximum_fusion.kv_ref
  11.2 0.0 copy-done.4
  11.2 0.6 broadcast_in_dim.12.sink_ref
  11.8 0.0 copy-done
  11.8 1.4 pad.9.w_ref
  13.2 63.2 %shard_map.140 = (bf16[4,8,40,2048]{3,2,1,0:T(8,128)(2,1)}, bf16[64,2048]{1,0:T(8,128)(2,1)}) custom-call(bf16[8,40,2048]{2,1,0:T(8,128)(2,1)} %bitcast.30, bf16[3,256,128]{2,1,0:T(8,128)(2,1)} %pad.8.q_ref, bf16[256,128]{1,0:T(8,128)(2,1)} %pad_maximum_fusion.kv_ref, f32[3,128]{1,0:T(4,128)} %broadcast_in_dim.12.sink_ref, bf16[3,128,2048]{2,1,0:T(8,128)(2,1)} %pad.9.w_ref, ...), custom_call_target="tpu_custom_call" | custom-call | tf_op jit(solution)/shard_map/pallas_call | solution.py:167
  76.4 0.0 copy-start.5
  76.4 0.0 copy-start.6
  76.4 8.7 %fusion.1 = f32[1280,896]{1,0:T(8,128)S(1)} fusion(bf16[1280,2048]{1,0:T(8,128)(2,1)} %bitcast.37, bf16[1,2048,896]{2,1,0:T(8,128)(2,1)} %param.23), kind=kOutput, calls=%fused_computation.2 | convolution fusion | flops 4697620480 | bytes 13500416 | tf_op jit(solution)/shard_map/dot_general | solution.py:305
  85.1 0.0 copy-done.5
  85.2 0.0 copy-done.6
  85.2 6.9 %multiply_convert_fusion = bf16[1280,896]{1,0:T(8,128)(2,1)} fusion(f32[1280,896]{1,0:T(8,128)S(1)} %fusion.1, bf16[1280,2048]{1,0:T(8,128)(2,1)S(1)} %bitcast.38, bf16[1,2048,896]{2,1,0:T(8,128)(2,1)S(1)} %copy-done.6), kind=kOutput, calls=%fused_computation | convolution fusion | flops 4704501760 | bytes 15794176 | tf_op jit(solution)/shard_map/dot_general | solution.py:306
  92.1 0.0 copy-start.3
  92.1 43.5 %shard_map.141 = bf16[8,40,2048]{2,1,0:T(8,128)(2,1)} custom-call(bf16[4,320,896]{2,1,0:T(8,128)(2,1)} %bitcast.32, bf16[896,2048]{1,0:T(8,128)(2,1)} %bitcast.31), custom_call_target="tpu_custom_call" | custom-call | tf_op jit(solution)/shard_map/pallas_call | solution.py:253
  135.6 0.0 copy-start.1
  135.6 0.0 copy-done.3
  135.6 1.8 %fusion.12 = f32[128,2048]{1,0:T(8,128)S(1)} fusion(bf16[320,2048]{1,0:T(8,128)(2,1)} %bitcast.28, f32[128,320]{0,1:T(8,128)S(1)} %select_reduce_fusion), kind=kOutput, calls=%fused_computation.22 | convolution fusion | flops 167813120 | bytes 2523136 | tf_op jit(solution)/shard_map/dot_general | solution.py:314
  137.5 2.6 %fusion.3 = bf16[128,2048]{1,0:T(8,128)(2,1)} fusion(f32[128,2048]{1,0:T(8,128)S(1)} %fusion.12, bf16[320,2048]{1,0:T(8,128)(2,1)} %bitcast.29, f32[128,320]{0,1:T(8,128)S(1)} %select_reduce_fusion), kind=kOutput, calls=%fused_computation.6 | convolution fusion | flops 168460288 | bytes 3047424 | tf_op jit(solution)/shard_map/dot_general | solution.py:314
  140.0 0.0 copy-done.1
  140.1 0.7 copy.44
  (6 shorter events, 0.1 us)
Async XLA Ops:
  0.6 9.7 %copy-start.2 = (bf16[256,64]{0,1:T(8,128)(2,1)S(1)}, bf16[256,64]{0,1:T(8,128)(2,1)}, u32[]{:S(2)}) copy-start(bf16[256,64]{0,1:T(8,128)(2,1)} %param.14) | copy-start | bytes 98308
  0.6 10.5 %copy-start.4 = (f32[3]{0:T(128)S(1)}, f32[3]{0:T(128)}, u32[]{:S(2)}) copy-start(f32[3]{0:T(128)} %param.16) | copy-start | bytes 40
  0.7 11.2 %copy-start = (bf16[192,2048]{1,0:T(8,128)(2,1)S(1)}, bf16[192,2048]{1,0:T(8,128)(2,1)}, u32[]{:S(2)}) copy-start(bf16[192,2048]{1,0:T(8,128)(2,1)} %param.17) | copy-start | bytes 2359300
  76.4 8.8 %copy-start.5 = (bf16[4,8,40,2048]{3,2,1,0:T(8,128)(2,1)S(1)}, bf16[4,8,40,2048]{3,2,1,0:T(8,128)(2,1)}, u32[]{:S(2)}) copy-start(bf16[4,8,40,2048]{3,2,1,0:T(8,128)(2,1)} %get-tuple-element.5) | copy-start | bytes 15728644
  76.4 8.8 %copy-start.6 = (bf16[1,2048,896]{2,1,0:T(8,128)(2,1)S(1)}, bf16[1,2048,896]{2,1,0:T(8,128)(2,1)}, u32[]{:S(2)}) copy-start(bf16[1,2048,896]{2,1,0:T(8,128)(2,1)} %param.24) | copy-start | bytes 11010052
  92.1 43.5 %copy-start.3 = (f32[128,2]{0,1:T(2,128)S(1)}, f32[128,2]{0,1:T(2,128)}, u32[]{:S(2)}) copy-start(f32[128,2]{0,1:T(2,128)} %param.22) | copy-start | bytes 3076
  135.6 4.5 %copy-start.1 = (bf16[64,2048]{1,0:T(8,128)(2,1)S(1)}, bf16[64,2048]{1,0:T(8,128)(2,1)}, u32[]{:S(2)}) copy-start(bf16[64,2048]{1,0:T(8,128)(2,1)} %get-tuple-element.8) | copy-start | bytes 786436

commit v3 on v2

--- a/solution.py
+++ b/solution.py
@@ -75,7 +75,7 @@
         kv_ref.at[pl.ds(tok_rows - WINDOW, WINDOW)], kv_prev,
         send_m.at[0], recv_m.at[0], (lax.rem(ep + 1, n), tp),
     )
-    order = far_first(n)
+    order = far_first(n)[::-1]
     direct = {}
     own = out_ref.at[ep]
     crossed = {0: send(own, slots.at[2, 0], send_x.at[0], recv_x.at[0], (ep, cross))}

time: 141 us -> 133 us (0.943)
  Pallas kernels: 107 us -> 98.2 us
    pallas_call x1, Pallas kernels: 63.2 us -> 52.9 us  [dispatch(): pl.pallas_call(functools.partial(dispatch_kernel, n), out_shape=(jax.Shap...]
    pallas_call x1, Pallas kernels: 43.5 us -> 45.3 us  [combine(): pl.pallas_call(functools.partial(combine_kernel, n), out_shape=jax.ShapeD...]
where the time goes in v3:
time: 133 us; the launch traced here: 132 us
  Pallas kernels  98.2 us (74%)
  matrix products  22.7 us (17%)
  local copies, waits for them, and re-layouts  7.02 us (5%)
  other arithmetic  3.55 us (3%)
    pallas_call x1, Pallas kernels, dispatch(): pl.pallas_call(functools.partial(dispatch_kernel, n), out_shape=(jax.Shap...  52.9 us
    pallas_call x1, Pallas kernels, combine(): pl.pallas_call(functools.partial(combine_kernel, n), out_shape=jax.ShapeD...  45.3 us
    dot_general x1, matrix products, shards(): jnp.dot(slot_rows, expert_gate[0], preferred_element_type=jnp.float32)  8.74 us
    dot_general x1, matrix products, shards(): jnp.dot(slot_rows, expert_up[0], preferred_element_type=jnp.float32)  6.92 us
    dot_general x1, matrix products, shards(): outgoing = jnp.dot(select_rows, normed, preferred_element_type=jnp.float32)  2.69 us

profile of v3, /device:TPU:0, one launch (start us, length us, event | category | flops | bytes accessed | tf_op | source)
XLA Modules:
  0.0 132.3 jit_solution(11823658199093564245)
XLA Ops:
  0.6 0.0 copy-start.2
  0.6 0.0 copy-start.4
  0.7 0.0 copy-start
  0.7 1.3 fusion.4
  2.0 0.8 copy.37
  2.8 0.1 eq.55
  2.9 0.6 reduce-window.6
  3.5 0.2 slice_reduce_fusion
  3.8 0.1 eq.51
  3.9 0.1 fusion.15
  4.0 0.1 reduce_sum.39
  4.1 0.1 copy.39
  4.2 0.7 multiply_add_fusion
  5.0 2.7 %convolution_convert_fusion = bf16[320,2048]{1,0:T(8,128)(2,1)} fusion(bf16[128,2048]{1,0:T(8,128)(2,1)} %param.19, f32[2048]{0:T(1024)} %param.20, f32[128]{0:T(128)S(1)} %add_rsqrt_fusion, bf16[320,128]{1,0:T(8,128)(2,1)S(1)} %convert_reduce_fusion), kind=kOutput, calls=%fused_computation.4 | convolution fusion | flops 169476096 | bytes 1925632 | tf_op jit(solution)/shard_map/dot_general | solution.py:293
  7.6 1.1 copy.40
  8.7 0.7 pad.8.q_ref
  9.4 0.9 copy.42
  10.3 0.0 copy-done.2
  10.3 0.1 copy.41
  10.4 0.7 pad_maximum_fusion.kv_ref
  11.2 0.0 copy-done.4
  11.2 0.6 broadcast_in_dim.12.sink_ref
  11.8 0.0 copy-done
  11.8 1.4 %pad.9.w_ref = bf16[3,128,2048]{2,1,0:T(8,128)(2,1)} pad(bf16[3,64,2048]{2,1,0:T(8,128)(2,1)S(1)} %bitcast.33, bf16[]{:T(256)} %constant.18.clone.1), padding=0_0x64_0x0_0 | pad | bytes 2359298 | tf_op jit(solution)/shard_map/jit(_pad)/pad | solution.py:300
  13.2 52.9 %shard_map.140 = (bf16[4,8,40,2048]{3,2,1,0:T(8,128)(2,1)}, bf16[64,2048]{1,0:T(8,128)(2,1)}) custom-call(bf16[8,40,2048]{2,1,0:T(8,128)(2,1)} %bitcast.30, bf16[3,256,128]{2,1,0:T(8,128)(2,1)} %pad.8.q_ref, bf16[256,128]{1,0:T(8,128)(2,1)} %pad_maximum_fusion.kv_ref, f32[3,128]{1,0:T(4,128)} %broadcast_in_dim.12.sink_ref, bf16[3,128,2048]{2,1,0:T(8,128)(2,1)} %pad.9.w_ref, ...), custom_call_target="tpu_custom_call" | custom-call | tf_op jit(solution)/shard_map/pallas_call | solution.py:167
  66.1 0.0 copy-start.5
  66.1 0.0 copy-start.6
  66.1 8.7 %fusion.1 = f32[1280,896]{1,0:T(8,128)S(1)} fusion(bf16[1280,2048]{1,0:T(8,128)(2,1)} %bitcast.37, bf16[1,2048,896]{2,1,0:T(8,128)(2,1)} %param.23), kind=kOutput, calls=%fused_computation.2 | convolution fusion | flops 4697620480 | bytes 13500416 | tf_op jit(solution)/shard_map/dot_general | solution.py:305
  74.9 0.0 copy-done.5
  74.9 0.0 copy-done.6
  74.9 6.9 %multiply_convert_fusion = bf16[1280,896]{1,0:T(8,128)(2,1)} fusion(f32[1280,896]{1,0:T(8,128)S(1)} %fusion.1, bf16[1280,2048]{1,0:T(8,128)(2,1)S(1)} %bitcast.38, bf16[1,2048,896]{2,1,0:T(8,128)(2,1)S(1)} %copy-done.6), kind=kOutput, calls=%fused_computation | convolution fusion | flops 4704501760 | bytes 15794176 | tf_op jit(solution)/shard_map/dot_general | solution.py:306
  81.8 0.0 copy-start.3
  81.8 45.3 %shard_map.141 = bf16[8,40,2048]{2,1,0:T(8,128)(2,1)} custom-call(bf16[4,320,896]{2,1,0:T(8,128)(2,1)} %bitcast.32, bf16[896,2048]{1,0:T(8,128)(2,1)} %bitcast.31), custom_call_target="tpu_custom_call" | custom-call | tf_op jit(solution)/shard_map/pallas_call | solution.py:253
  127.1 0.0 copy-start.1
  127.1 0.0 copy-done.3
  127.2 1.8 %fusion.12 = f32[128,2048]{1,0:T(8,128)S(1)} fusion(bf16[320,2048]{1,0:T(8,128)(2,1)} %bitcast.28, f32[128,320]{0,1:T(8,128)S(1)} %select_reduce_fusion), kind=kOutput, calls=%fused_computation.22 | convolution fusion | flops 167813120 | bytes 2523136 | tf_op jit(solution)/shard_map/dot_general | solution.py:314
  129.0 2.6 %fusion.3 = bf16[128,2048]{1,0:T(8,128)(2,1)} fusion(f32[128,2048]{1,0:T(8,128)S(1)} %fusion.12, bf16[320,2048]{1,0:T(8,128)(2,1)} %bitcast.29, f32[128,320]{0,1:T(8,128)S(1)} %select_reduce_fusion), kind=kOutput, calls=%fused_computation.6 | convolution fusion | flops 168460288 | bytes 3047424 | tf_op jit(solution)/shard_map/dot_general | solution.py:314
  131.6 0.0 copy-done.1
  131.6 0.7 copy.44
  (6 shorter events, 0.1 us)
Async XLA Ops:
  0.6 9.7 %copy-start.2 = (bf16[256,64]{0,1:T(8,128)(2,1)S(1)}, bf16[256,64]{0,1:T(8,128)(2,1)}, u32[]{:S(2)}) copy-start(bf16[256,64]{0,1:T(8,128)(2,1)} %param.14) | copy-start | bytes 98308
  0.6 10.5 %copy-start.4 = (f32[3]{0:T(128)S(1)}, f32[3]{0:T(128)}, u32[]{:S(2)}) copy-start(f32[3]{0:T(128)} %param.16) | copy-start | bytes 40
  0.7 11.2 %copy-start = (bf16[192,2048]{1,0:T(8,128)(2,1)S(1)}, bf16[192,2048]{1,0:T(8,128)(2,1)}, u32[]{:S(2)}) copy-start(bf16[192,2048]{1,0:T(8,128)(2,1)} %param.17) | copy-start | bytes 2359300
  66.1 8.8 %copy-start.5 = (bf16[4,8,40,2048]{3,2,1,0:T(8,128)(2,1)S(1)}, bf16[4,8,40,2048]{3,2,1,0:T(8,128)(2,1)}, u32[]{:S(2)}) copy-start(bf16[4,8,40,2048]{3,2,1,0:T(8,128)(2,1)} %get-tuple-element.5) | copy-start | bytes 15728644
  66.1 8.8 %copy-start.6 = (bf16[1,2048,896]{2,1,0:T(8,128)(2,1)S(1)}, bf16[1,2048,896]{2,1,0:T(8,128)(2,1)}, u32[]{:S(2)}) copy-start(bf16[1,2048,896]{2,1,0:T(8,128)(2,1)} %param.24) | copy-start | bytes 11010052
  81.8 45.3 %copy-start.3 = (f32[128,2]{0,1:T(2,128)S(1)}, f32[128,2]{0,1:T(2,128)}, u32[]{:S(2)}) copy-start(f32[128,2]{0,1:T(2,128)} %param.22) | copy-start | bytes 3076
  127.1 4.5 %copy-start.1 = (bf16[64,2048]{1,0:T(8,128)(2,1)S(1)}, bf16[64,2048]{1,0:T(8,128)(2,1)}, u32[]{:S(2)}) copy-start(bf16[64,2048]{1,0:T(8,128)(2,1)} %get-tuple-element.8) | copy-start | bytes 786436
